TPU v7x, 32 devices: a whole 2x2x4 slice. The times are simulated.
32 devices in a mesh: rep: 2 (over x), fs: 8 (over z, y), tp: 2 (over core).
Axes of the slice: x: 2, y: 2, z: 4, core: 2. Of those that a mesh axis runs over, the one named last changes fastest.
Arguments:
- tokens: bfloat16 [4096, 2048], P(('rep', 'fs')), may hold values from -6 to 6
- ffn_gate: bfloat16 [2048, 5632], P('fs', 'tp'), may hold values from -0.125 to 0.125
- ffn_up: bfloat16 [2048, 5632], P('fs', 'tp'), may hold values from -0.125 to 0.125
- ffn_down: bfloat16 [5632, 2048], P('tp', 'fs'), may hold values from -0.3125 to 0.3125
- query_proj: bfloat16 [2048, 512], P('fs', 'tp'), may hold values from -0.125 to 0.125
- key_proj: bfloat16 [2048, 512], P('fs', 'tp'), may hold values from -0.125 to 0.125
- value_proj: bfloat16 [2048, 1024], P('fs', 'tp'), may hold values from -0.125 to 0.125
- outgate_proj: bfloat16 [2048, 1024], P('fs', 'tp'), may hold values from -0.125 to 0.125
- output_proj: bfloat16 [1024, 2048], P('tp', 'fs'), may hold values from -0.375 to 0.375
- rank_down: bfloat16 [2048, 16], replicated, may hold values from -0.1875 to 0.1875
- rank_up: bfloat16 [16, 512], replicated, may hold values from -3 to 3
- decay_bias: float32 [512], replicated, may hold values from -0.5 to 8
- head_gain: float32 [1024], replicated, may hold values from 0.1 to 1.9
- norm_gain: float32 [3, 2048], replicated, may hold values from 0.1 to 1.9
- norm_bias: float32 [3, 2048], replicated, may hold values from -2 to 2
Outputs:
- layer_out: bfloat16 [4096, 2048], P(('rep', 'fs'))
All inputs are finite; a program needn't handle non-finite values.
Results may differ from a plain program's by a relative error of at most 0.024.
Values may be sent and summed in bfloat16 or wider, within the bound.
A program may use at most 128 MiB of HBM per device.

v0:
```python
import jax
import jax.numpy as jnp
from jax import lax
from jax.sharding import PartitionSpec as P

DK = 64
DV = 128
BLOCK = 64


EPSILON = 1e-05
HEAD_FLOOR = 1.0
RESIDUAL_SCALE = 2.0**0.5
GATE_SOFTNESS = 16.0
FULL_ACCURACY = lax.Precision.HIGHEST


def layer_norm(summed, norm_gain, norm_shift):
    centred = summed - jnp.mean(summed, -1, keepdims=True)
    spread = jnp.mean(centred * centred, -1, keepdims=True)
    return (centred * lax.rsqrt(spread + EPSILON) * norm_gain + norm_shift).astype(jnp.bfloat16)


def gla_heads(queries, keys_rows, values, decay_logarithm):
    length, head_count, key_width = queries.shape
    value_width = values.shape[-1]
    block_count = length // BLOCK

    def blocks(array):
        return array.reshape(block_count, BLOCK, head_count, array.shape[-1])

    causal = jnp.tril(jnp.ones((BLOCK, BLOCK), bool))[:, :, None, None]

    def advance(running_state, inputs):
        query_block, key_block, value_block, decay_blk = inputs
        decay_prefix = jnp.cumsum(decay_blk, axis=0)
        spread = decay_prefix[:, None] - decay_prefix[None, :]
        weight = jnp.exp(jnp.where(causal, spread, -jnp.inf))
        scores = jnp.einsum(
            "lshk,lhk,shk->hls", weight, query_block, key_block, precision=FULL_ACCURACY
        )
        within = jnp.einsum("hls,shv->lhv", scores, value_block, precision=FULL_ACCURACY)
        carried_over = jnp.einsum(
            "zew,ewa->zea",
            query_block * jnp.exp(decay_prefix),
            running_state,
            precision=FULL_ACCURACY,
        )
        block_finish = decay_prefix[-1]
        running_state = jnp.exp(block_finish)[:, :, None] * running_state + jnp.einsum(
            "oct,ocy->cty",
            key_block * jnp.exp(block_finish[None] - decay_prefix),
            value_block,
            precision=FULL_ACCURACY,
        )
        return (running_state, within + carried_over)

    initial = jnp.zeros((head_count, key_width, value_width), jnp.float32)
    _, outputs = lax.scan(
        advance,
        initial,
        (blocks(queries), blocks(keys_rows), blocks(values), blocks(decay_logarithm)),
    )
    return outputs.reshape(length, head_count, value_width)


def settle(partial_value, residual_rows, factor, norm_gain, norm_shift):
    summed = lax.psum(partial_value.astype(jnp.bfloat16), "tp").astype(jnp.float32)
    return layer_norm(
        RESIDUAL_SCALE * residual_rows.astype(jnp.float32) + factor * summed, norm_gain, norm_shift
    )


def channel_mix(normed, gate_full, up_full, down_full):
    gate_rows = jnp.dot(normed, gate_full, preferred_element_type=jnp.float32)
    up_rows = jnp.dot(normed, up_full, preferred_element_type=jnp.float32)
    hidden = (jax.nn.silu(gate_rows) * up_rows).astype(jnp.bfloat16)
    return jnp.dot(hidden, down_full, preferred_element_type=jnp.float32)


def per_device(
    tokens,
    ffn_gate,
    ffn_up,
    ffn_down,
    query_proj,
    key_proj,
    value_proj,
    outgate_proj,
    output_proj,
    rank_down,
    rank_up,
    decay_bias,
    head_gain,
    norm_gain,
    norm_bias,
):
    row_count = tokens.shape[0]
    gate_full, up_full = (
        lax.all_gather(ffn_gate, "fs", axis=0, tiled=True),
        lax.all_gather(ffn_up, "fs", axis=0, tiled=True),
    )
    down_full = lax.all_gather(ffn_down, "fs", axis=1, tiled=True)
    first_partial = channel_mix(tokens, gate_full, up_full, down_full)
    first = settle(first_partial, tokens, 0.5, norm_gain[0], norm_bias[0])
    key_cols = query_proj.shape[1]
    value_cols = value_proj.shape[1]
    query_full, key_full, value_full, outgate_full = (
        lax.all_gather(query_proj, "fs", axis=0, tiled=True),
        lax.all_gather(key_proj, "fs", axis=0, tiled=True),
        lax.all_gather(value_proj, "fs", axis=0, tiled=True),
        lax.all_gather(outgate_proj, "fs", axis=0, tiled=True),
    )
    joined_full = jnp.concatenate([query_full, key_full, value_full, outgate_full], axis=1)
    projected = jnp.dot(first, joined_full, preferred_element_type=jnp.float32)
    queries = projected[:, :key_cols] * DK ** (-0.5)
    keys_rows = projected[:, key_cols : 2 * key_cols]
    values = projected[:, 2 * key_cols : 2 * key_cols + value_cols]
    gates = projected[:, 2 * key_cols + value_cols :]
    head_count = key_cols // DK
    position = lax.axis_index("tp")
    key_start = position * (head_count * DK)
    value_start = position * (head_count * DV)
    rank_rows = jnp.dot(first, rank_down, preferred_element_type=jnp.float32)
    up_block = lax.dynamic_slice_in_dim(rank_up, key_start, head_count * DK, 1).astype(jnp.float32)
    bias_block = lax.dynamic_slice_in_dim(decay_bias, key_start, head_count * DK, 0)
    decay_source = jnp.dot(rank_rows, up_block, precision=FULL_ACCURACY) + bias_block
    decay_logarithm = jax.nn.log_sigmoid(decay_source) / GATE_SOFTNESS
    heads_out = gla_heads(
        queries.reshape(row_count, head_count, DK),
        keys_rows.reshape(row_count, head_count, DK),
        values.reshape(row_count, head_count, DV),
        decay_logarithm.reshape(row_count, head_count, DK),
    )
    scaled = heads_out * lax.rsqrt(jnp.mean(heads_out * heads_out, -1, keepdims=True) + HEAD_FLOOR)
    gain_block = lax.dynamic_slice_in_dim(head_gain, value_start, head_count * DV, 0)
    scaled = scaled * gain_block.reshape(head_count, DV)
    mixed = (scaled.reshape(row_count, head_count * DV) * jax.nn.silu(gates)).astype(jnp.bfloat16)
    mixer_partial = jnp.dot(
        mixed,
        lax.all_gather(output_proj, "fs", axis=1, tiled=True),
        preferred_element_type=jnp.float32,
    )
    second = settle(mixer_partial, first, 1.0, norm_gain[1], norm_bias[1])
    third_partial = channel_mix(second, gate_full, up_full, down_full)
    return settle(third_partial, second, 0.5, norm_gain[2], norm_bias[2])


def solution(mesh):
    return jax.shard_map(
        per_device,
        mesh=mesh,
        in_specs=(
            P(("rep", "fs"), None),
            P("fs", "tp"),
            P("fs", "tp"),
            P("tp", "fs"),
            P("fs", "tp"),
            P("fs", "tp"),
            P("fs", "tp"),
            P("fs", "tp"),
            P("tp", "fs"),
            P(),
            P(),
            P(),
            P(),
            P(),
            P(),
        ),
        out_specs=P(("rep", "fs"), None),
        check_vma=False,
    )
```

profile of v0, /device:TPU:25, one launch (start us, length us, event | category | flops | bytes accessed | tf_op | source)
XLA Modules:
  0.0 916.6 jit_solution(16187257873956331330)
XLA Ops:
  8.8 163.2 %all-gather.9.cloned.1.call-done = bf16[2048,2816]{1,0:T(8,128)(2,1)} async-done(((bf16[256,2816]{1,0:T(8,128)(2,1)}), bf16[2048,2816]{1,0:T(8,128)(2,1)}) %all-gather.9.cloned.1.call-update) | async-done | bytes 11534352 | tf_op jit(solution)/shard_map/all_gather | solution.py:100
  172.0 9.0 fusion.50
  181.1 154.7 %all-gather.11.cloned.1.call-done = bf16[2048,2816]{1,0:T(8,128)(2,1)} async-done(((bf16[256,2816]{1,0:T(8,128)(2,1)}), bf16[2048,2816]{1,0:T(8,128)(2,1)}) %all-gather.11.cloned.1.call-update) | async-done | bytes 11534352 | tf_op jit(solution)/shard_map/all_gather | solution.py:101
  335.7 163.6 %all-gather.13.cloned.1.call-done = bf16[2816,2048]{1,0:T(8,128)(2,1)} async-done(((bf16[2816,256]{1,0:T(8,128)(2,1)}), bf16[2816,2048]{1,0:T(8,128)(2,1)}) %all-gather.13.cloned.1.call-update) | async-done | bytes 11534352 | tf_op jit(solution)/shard_map/all_gather | solution.py:103
  499.3 15.5 %convolution_convert_fusion.2 = bf16[256,2048]{1,0:T(8,128)(2,1)} fusion(bf16[2816,2048]{1,0:T(8,128)(2,1)} %all-gather.13.cloned.1.call-done, bf16[256,2048]{1,0:T(8,128)(2,1)S(1)} %copy-done.2, bf16[2048,2816]{1,0:T(8,128)(2,1)} %all-gather.11.cloned.1.call-done, f32[256,2816]{1,0:T(8,128)} %fusion.50), kind=kOutput, calls=%fused_computation.45 | convolution fusion | flops 5910429696 | bytes 28049408 | tf_op jit(solution)/shard_map/dot_general | solution.py:78
  518.3 14.4 %all-reduce.6.cloned.1.call-start = ((), (), s32[]{:S(2)}) async-start(), calls=%async_computation.9 | async-start | bytes 2097152 | tf_op jit(solution)/shard_map/psum | solution.py:68
  538.4 36.3 %all-gather.15.cloned.1.call-done = bf16[2048,256]{1,0:T(8,128)(2,1)} async-done(((bf16[256,256]{1,0:T(8,128)(2,1)}), bf16[2048,256]{1,0:T(8,128)(2,1)}) %all-gather.15.cloned.1.call-update) | async-done | bytes 1048592 | tf_op jit(solution)/shard_map/all_gather | solution.py:109
  574.6 41.0 %all-gather.17.cloned.1.call-done = bf16[2048,256]{1,0:T(8,128)(2,1)} async-done(((bf16[256,256]{1,0:T(8,128)(2,1)}), bf16[2048,256]{1,0:T(8,128)(2,1)}) %all-gather.17.cloned.1.call-update) | async-done | bytes 1048592 | tf_op jit(solution)/shard_map/all_gather | solution.py:110
  615.6 51.3 %all-gather.19.cloned.1.call-done = bf16[2048,512]{1,0:T(8,128)(2,1)} async-done(((bf16[256,512]{1,0:T(8,128)(2,1)}), bf16[2048,512]{1,0:T(8,128)(2,1)}) %all-gather.19.cloned.1.call-update) | async-done | bytes 2097168 | tf_op jit(solution)/shard_map/all_gather | solution.py:111
  666.9 49.8 %all-gather.21.cloned.1.call-done = bf16[2048,512]{1,0:T(8,128)(2,1)} async-done(((bf16[256,512]{1,0:T(8,128)(2,1)}), bf16[2048,512]{1,0:T(8,128)(2,1)}) %all-gather.21.cloned.1.call-update) | async-done | bytes 2097168 | tf_op jit(solution)/shard_map/all_gather | solution.py:112
  716.7 3.9 fusion.20
  723.9 105.8 %while.13 = (s32[]{:T(128)}, f32[4,64,128]{2,1,0:T(8,128)S(1)}, f32[4,64,4,128]{3,1,2,0:T(8,128)}, f32[4,64,4,64]{3,2,1,0:T(4,128)S(1)}, f32[4,64,4,64]{3,2,1,0:...) while((s32[]{:T(128)}, f32[4,64,128]{2,1,0:T(8,128)S(1)}, ...), condition=%wide.region_5.6_spmd.clone, body=%wide.region_3.5_spmd.clone.sunk | while | flops 92475392 | bytes 10893944 | solution.py:59
  725.0 5.9 multiply_bitcast_fusion.2
  730.9 17.6 %fusion.91 = f32[4,64,1,64]{3,2,1,0:T(1,128)S(1)} fusion(f32[64,4,64,64]{2,1,3,0:T(4,128)S(1)} %multiply_bitcast_fusion.2, f32[64,4,64,1]{2,1,0,3:T(4,128)S(1)} %dynamic-slice_bitcast_fusion.4), kind=kOutput, calls=%fused_computation.1.clone.1 | convolution fusion | flops 12582912 | bytes 4325376 | tf_op jit(solution)/shard_map/while/body/eval_jaxpr/lshk,lhk,shk->hls/dot_general | solution.py:39
  751.4 5.9 multiply_bitcast_fusion.2
  757.3 17.6 %fusion.91 = f32[4,64,1,64]{3,2,1,0:T(1,128)S(1)} fusion(f32[64,4,64,64]{2,1,3,0:T(4,128)S(1)} %multiply_bitcast_fusion.2, f32[64,4,64,1]{2,1,0,3:T(4,128)S(1)} %dynamic-slice_bitcast_fusion.4), kind=kOutput, calls=%fused_computation.1.clone.1 | convolution fusion | flops 12582912 | bytes 4325376 | tf_op jit(solution)/shard_map/while/body/eval_jaxpr/lshk,lhk,shk->hls/dot_general | solution.py:39
  777.8 5.9 multiply_bitcast_fusion.2
  783.7 17.6 %fusion.91 = f32[4,64,1,64]{3,2,1,0:T(1,128)S(1)} fusion(f32[64,4,64,64]{2,1,3,0:T(4,128)S(1)} %multiply_bitcast_fusion.2, f32[64,4,64,1]{2,1,0,3:T(4,128)S(1)} %dynamic-slice_bitcast_fusion.4), kind=kOutput, calls=%fused_computation.1.clone.1 | convolution fusion | flops 12582912 | bytes 4325376 | tf_op jit(solution)/shard_map/while/body/eval_jaxpr/lshk,lhk,shk->hls/dot_general | solution.py:39
  804.2 5.9 multiply_bitcast_fusion.2
  810.1 17.6 %fusion.91 = f32[4,64,1,64]{3,2,1,0:T(1,128)S(1)} fusion(f32[64,4,64,64]{2,1,3,0:T(4,128)S(1)} %multiply_bitcast_fusion.2, f32[64,4,64,1]{2,1,0,3:T(4,128)S(1)} %dynamic-slice_bitcast_fusion.4), kind=kOutput, calls=%fused_computation.1.clone.1 | convolution fusion | flops 12582912 | bytes 4325376 | tf_op jit(solution)/shard_map/while/body/eval_jaxpr/lshk,lhk,shk->hls/dot_general | solution.py:39
  836.4 20.8 %all-reduce.6.cloned.1.call-done = bf16[256,2048]{1,0:T(8,128)(2,1)} async-done(((bf16[256,2048]{1,0:T(8,128)(2,1)}), bf16[256,2048]{1,0:T(8,128)(2,1)}) %all-reduce.6.cloned.1.call-update) | async-done | bytes 1048592 | tf_op jit(solution)/shard_map/psum | solution.py:68
  860.2 9.0 fusion.52
  869.3 15.5 %convolution_convert_fusion = bf16[256,2048]{1,0:T(8,128)(2,1)} fusion(bf16[2816,2048]{1,0:T(8,128)(2,1)} %all-gather.13.cloned.1.call-done, bf16[256,2048]{1,0:T(8,128)(2,1)S(1)} %add_convert_fusion.1, bf16[2048,2816]{1,0:T(8,128)(2,1)} %all-gather.11.cloned.1.call-done, f32[256,2816]{1,0:T(8,128)} %fusion.52), kind=kOutput, calls=%fused_computation.43 | convolution fusion | flops 5910429696 | bytes 28049408 | tf_op jit(solution)/shard_map/dot_general | solution.py:78
  884.8 20.8 %all-reduce.8.cloned.1.call-done = bf16[256,2048]{1,0:T(8,128)(2,1)} async-done(((bf16[256,2048]{1,0:T(8,128)(2,1)}), bf16[256,2048]{1,0:T(8,128)(2,1)}) %all-reduce.8.cloned.1.call-update) | async-done | bytes 1048592 | tf_op jit(solution)/shard_map/psum | solution.py:68
  (123 shorter events, 39.6 us)
Async XLA Ops:
  6.5 714.1 %copy-start = (bf16[2048,16]{0,1:T(8,128)(2,1)S(1)}, bf16[2048,16]{0,1:T(8,128)(2,1)}, u32[]{:S(2)}) copy-start(bf16[2048,16]{0,1:T(8,128)(2,1)} %param.26) | copy-start | bytes 196612
  6.5 165.5 %copy-start.2 = (bf16[256,2048]{1,0:T(8,128)(2,1)S(1)}, bf16[256,2048]{1,0:T(8,128)(2,1)}, u32[]{:S(2)}) copy-start(bf16[256,2048]{1,0:T(8,128)(2,1)} %param.17) | copy-start | bytes 3145732
  6.5 165.5 %all-gather.9.cloned.1.call-start = ((), (), s32[]{:S(2)}) async-start(), calls=%async_computation | async-start | bytes 12976128 | tf_op jit(solution)/shard_map/all_gather | solution.py:100
  7.3 328.5 %all-gather.11.cloned.1.call-start = ((), (), s32[]{:S(2)}) async-start(), calls=%async_computation.1 | async-start | bytes 12976128 | tf_op jit(solution)/shard_map/all_gather | solution.py:101
  8.0 491.3 %all-gather.13.cloned.1.call-start = ((), (), s32[]{:S(2)}) async-start(), calls=%async_computation.2 | async-start | bytes 12976128 | tf_op jit(solution)/shard_map/all_gather | solution.py:103
  8.7 526.5 %all-reduce.4.cloned.1.call-start = ((), (), s32[]{:S(2)}) async-start(), calls=%async_computation.3 | async-start | bytes 2097152 | tf_op jit(solution)/shard_map/psum | solution.py:68
  514.9 17.9 %copy-start.7 = (f32[3,2048]{1,0:T(4,128)S(1)}, f32[3,2048]{1,0:T(4,128)}, u32[]{:S(2)}) copy-start(f32[3,2048]{1,0:T(4,128)} %param.30) | copy-start | bytes 73732
  514.9 17.9 %copy-start.8 = (f32[3,2048]{1,0:T(4,128)S(1)}, f32[3,2048]{1,0:T(4,128)}, u32[]{:S(2)}) copy-start(f32[3,2048]{1,0:T(4,128)} %param.31) | copy-start | bytes 73732
  514.9 18.0 %copy-start.10 = (f32[512]{0:T(512)S(1)}, f32[512]{0:T(512)}, u32[]{:S(2)}) copy-start(f32[512]{0:T(512)} %param.28) | copy-start | bytes 6148
  514.9 18.0 %copy-start.9 = (f32[1024]{0:T(1024)S(1)}, f32[1024]{0:T(1024)}, u32[]{:S(2)}) copy-start(f32[1024]{0:T(1024)} %param.29) | copy-start | bytes 12292
  514.9 59.7 %all-gather.15.cloned.1.call-start = ((), (), s32[]{:S(2)}) async-start(), calls=%async_computation.4 | async-start | bytes 1179648 | tf_op jit(solution)/shard_map/all_gather | solution.py:109
  515.5 100.1 %all-gather.17.cloned.1.call-start = ((), (), s32[]{:S(2)}) async-start(), calls=%async_computation.5 | async-start | bytes 1179648 | tf_op jit(solution)/shard_map/all_gather | solution.py:110
  516.1 150.8 %all-gather.19.cloned.1.call-start = ((), (), s32[]{:S(2)}) async-start(), calls=%async_computation.6 | async-start | bytes 2359296 | tf_op jit(solution)/shard_map/all_gather | solution.py:111
  516.8 199.8 %all-gather.21.cloned.1.call-start = ((), (), s32[]{:S(2)}) async-start(), calls=%async_computation.7 | async-start | bytes 2359296 | tf_op jit(solution)/shard_map/all_gather | solution.py:112
  517.6 314.9 %all-gather.23.cloned.1.call-start = ((), (), s32[]{:S(2)}) async-start(), calls=%async_computation.8 | async-start | bytes 2359296 | tf_op jit(solution)/shard_map/all_gather | solution.py:141
  518.3 339.0 %all-reduce.6.cloned.1.call-start = ((), (), s32[]{:S(2)}) async-start(), calls=%async_computation.9 | async-start | bytes 2097152 | tf_op jit(solution)/shard_map/psum | solution.py:68
  535.2 1.8 copy-start.3
  720.5 1.2 copy-start.6
  720.5 1.2 copy-start.11
  722.2 1.5 slice-start
  836.4 69.2 %all-reduce.8.cloned.1.call-start = ((), (), s32[]{:S(2)}) async-start(), calls=%async_computation.10 | async-start | bytes 2097152 | tf_op jit(solution)/shard_map/psum | solution.py:68
  857.3 1.7 copy-start.4
  905.6 1.8 copy-start.5
  907.4 2.3 copy-start.1
Sparse Core Ops, SparseCore 0:
  9.5 162.4 all-gather.8
  174.2 161.4 all-gather.10
  337.8 161.4 all-gather.12
  515.0 20.1 all-reduce.3
  537.2 37.3 all-gather.14
  576.6 38.9 all-gather.16
  617.7 49.0 all-gather.18
  669.0 47.6 all-gather.20
  718.7 48.9 all-gather.22
  836.5 20.7 all-reduce.5
  885.0 20.5 all-reduce.7
where the time goes:
time: 929 us; the launch traced here: 917 us
  waiting for transfers between devices  709 us (76%)
  matrix products  135 us (15%)
  other arithmetic  39.5 us (4%)
  starting transfers between devices  14.8 us (2%)
  between operations  13.9 us (1%)
    all_gather x1, waiting for transfers between devices, per_device(): down_full = lax.all_gather(ffn_down, 'fs', axis=1, tiled=True)  164 us
    all_gather x1, waiting for transfers between devices, per_device(): lax.all_gather(ffn_gate, 'fs', axis=0, tiled=True)  163 us
    all_gather x1, waiting for transfers between devices, per_device(): lax.all_gather(ffn_up, 'fs', axis=0, tiled=True)  155 us
    dot_general x4, matrix products, advance(): jnp.einsum('lshk,lhk,shk->hls', weight, query_block, key_block, precision...  70.4 us
    all_gather x1, waiting for transfers between devices, per_device(): lax.all_gather(value_proj, 'fs', axis=0, tiled=True)  51.3 us
    all_gather x1, waiting for transfers between devices, per_device(): lax.all_gather(outgate_proj, 'fs', axis=0, tiled=True)  49.8 us
    psum x3, waiting for transfers between devices, settle(): lax.psum(partial_value.astype(jnp.bfloat16), 'tp').astype(jnp.float32)  43.8 us
    all_gather x1, waiting for transfers between devices, per_device(): lax.all_gather(key_proj, 'fs', axis=0, tiled=True)  41 us
  transfers between devices with their start and end apart: 11, of which 10 were waited for; matrix products, arithmetic and copies ran while one was open for 14% of the time, Pallas kernels for 0%

commit v1 on v0

v1 whole, which is shorter than its diff:
```python
import functools

import jax
import jax.numpy as jnp
from jax import lax
from jax.experimental import pallas as pl
from jax.experimental.pallas import tpu as pltpu
from jax.sharding import PartitionSpec as P

DK = 64
DV = 128
CHUNK = 16

EPSILON = 1e-05
HEAD_FLOOR = 1.0
RESIDUAL_SCALE = 2.0**0.5
GATE_SOFTNESS = 16.0
FULL_ACCURACY = lax.Precision.HIGHEST
MESH = pl.DeviceIdType.MESH
HBM = pl.BlockSpec(memory_space=pltpu.MemorySpace.HBM)
VMEM = pl.BlockSpec(memory_space=pltpu.MemorySpace.VMEM)


def gather_kernel(nz, ny, count, *refs):
    ins, outs = refs[:count], refs[count : 2 * count]
    send_main, recv_main, send_far, recv_far, local_sem = refs[2 * count :]
    rep = lax.axis_index("rep")
    fs = lax.axis_index("fs")
    z, y = fs // ny, fs % ny

    def place(dz, dy):
        return lax.rem(z + nz - dz, nz) * ny + lax.rem(y + ny - dy, ny)

    def peer(dz, dy):
        return lax.rem(z + dz, nz) * ny + lax.rem(y + dy, ny)

    partners = [{"fs": peer(dz, 0)} for dz in range(1, nz)]
    partners += [{"fs": peer(0, dy)} for dy in range(1, ny)]
    partners += [{"rep": 1 - rep}]
    barrier = pltpu.get_barrier_semaphore()
    for partner in partners:
        pl.semaphore_signal(barrier, inc=1, device_id=partner, device_id_type=MESH)
    pl.semaphore_wait(barrier, len(partners))

    def main_rows(at):
        rows = ins[at].shape[0]
        return pl.ds(pl.multiple_of(rep * (rows * 3 // 8), 8), rows * 5 // 8)

    def main_copy(at, dz, dy):
        rows = main_rows(at)
        over_y = dy > 0
        block = place(dz, 0) if over_y else fs
        source = outs[at].at[block, rows] if over_y and dz > 0 else ins[at].at[rows]
        return pltpu.make_async_remote_copy(
            src_ref=source,
            dst_ref=outs[at].at[block, rows],
            send_sem=send_main.at[at, dz, dy],
            recv_sem=recv_main.at[at, dz, dy],
            device_id={"fs": peer(0, dy) if over_y else peer(dz, 0)},
            device_id_type=MESH,
        )

    def main_landed(at, dz, dy):
        rows = main_rows(at)
        landed = outs[at].at[place(dz, dy), rows]
        return pltpu.make_async_remote_copy(
            src_ref=landed,
            dst_ref=landed,
            send_sem=send_main.at[at, dz, dy],
            recv_sem=recv_main.at[at, dz, dy],
            device_id={"fs": peer(dz, 0) if dy == 0 else peer(0, dy)},
            device_id_type=MESH,
        )

    def far_copy(at, dz, dy, rows):
        moved = outs[at].at[place(dz, dy), rows]
        return pltpu.make_async_remote_copy(
            src_ref=moved,
            dst_ref=moved,
            send_sem=send_far.at[at, dz, dy],
            recv_sem=recv_far.at[at, dz, dy],
            device_id={"rep": 1 - rep},
            device_id_type=MESH,
        )

    def own_far_rows(at):
        rows = ins[at].shape[0]
        return pl.ds(pl.multiple_of(rep * (rows * 5 // 8), 8), rows * 3 // 8)

    def other_far_rows(at):
        rows = ins[at].shape[0]
        return pl.ds(pl.multiple_of((1 - rep) * (rows * 5 // 8), 8), rows * 3 // 8)

    started = []
    locals_ = []
    for at in range(count):
        for dz in range(1, nz):
            copy = main_copy(at, dz, 0)
            copy.start()
            started.append(copy)
        for dy in range(1, ny):
            copy = main_copy(at, 0, dy)
            copy.start()
            started.append(copy)
        copy = pltpu.make_async_copy(ins[at], outs[at].at[fs], local_sem.at[at])
        copy.start()
        locals_.append(copy)

    def after_z(at):
        for dz in range(1, nz):
            main_landed(at, dz, 0).wait_recv()
            for dy in range(1, ny):
                copy = main_copy(at, dz, dy)
                copy.start()
                started.append(copy)
            copy = far_copy(at, dz, 0, own_far_rows(at))
            copy.start()
            started.append(copy)

    def after_y(at):
        for dz in range(nz):
            for dy in range(1, ny):
                main_landed(at, dz, dy).wait_recv()
                copy = far_copy(at, dz, dy, own_far_rows(at))
                copy.start()
                started.append(copy)

    for at in range(count + 1):
        if at < count:
            after_z(at)
        if at > 0:
            after_y(at - 1)
    for at in range(count):
        for dz in range(nz):
            for dy in range(ny):
                if dz or dy:
                    far_copy(at, dz, dy, other_far_rows(at)).wait_recv()
    for copy in started:
        copy.wait_send()
    for copy in locals_:
        copy.wait()


def gather_all(mesh_shape, shards):
    n = mesh_shape["fs"]
    ny = 2 ** ((n.bit_length() - 1) // 2)
    nz = n // ny
    count = len(shards)
    semaphores = pltpu.SemaphoreType.DMA((count, nz, ny))
    return pl.pallas_call(
        functools.partial(gather_kernel, nz, ny, count),
        out_shape=[jax.ShapeDtypeStruct((n, *shard.shape), shard.dtype) for shard in shards],
        in_specs=[VMEM] * count,
        out_specs=[HBM] * count,
        scratch_shapes=[semaphores] * 4 + [pltpu.SemaphoreType.DMA((count,))],
        compiler_params=pltpu.CompilerParams(collective_id=0, has_side_effects=True),
        name="gather_weights",
    )(*shards)


def settle_kernel(ntp, factor, part_ref, rest_ref, gain_ref, shift_ref, out_ref, got, send, recv):
    tp = lax.axis_index("tp")
    barrier = pltpu.get_barrier_semaphore()
    for d in range(1, ntp):
        pl.semaphore_signal(
            barrier, inc=1, device_id={"tp": lax.rem(tp + d, ntp)}, device_id_type=MESH
        )
    pl.semaphore_wait(barrier, ntp - 1)
    copies = []
    for d in range(1, ntp):
        copy = pltpu.make_async_remote_copy(
            src_ref=part_ref,
            dst_ref=got.at[d - 1],
            send_sem=send.at[d - 1],
            recv_sem=recv.at[d - 1],
            device_id={"tp": lax.rem(tp + d, ntp)},
            device_id_type=MESH,
        )
        copy.start()
        copies.append(copy)
    for copy in copies:
        copy.wait()
    tile = 16

    def one(step, carry):
        rows = pl.ds(pl.multiple_of(step * tile, tile), tile)
        summed = part_ref[rows, :].astype(jnp.float32)
        for d in range(ntp - 1):
            summed = summed + got[d, rows, :].astype(jnp.float32)
        summed = RESIDUAL_SCALE * rest_ref[rows, :].astype(jnp.float32) + factor * summed
        centred = summed - jnp.mean(summed, -1, keepdims=True)
        spread = jnp.mean(centred * centred, -1, keepdims=True)
        normed = centred * lax.rsqrt(spread + EPSILON) * gain_ref[...] + shift_ref[...]
        out_ref[rows, :] = normed.astype(jnp.bfloat16)
        return carry

    lax.fori_loop(0, part_ref.shape[0] // tile, one, 0)


def settle(ntp, which, partial_value, residual_rows, factor, norm_gain, norm_bias):
    rows, width = partial_value.shape
    return pl.pallas_call(
        functools.partial(settle_kernel, ntp, factor),
        out_shape=jax.ShapeDtypeStruct((rows, width), jnp.bfloat16),
        in_specs=[VMEM] * 4,
        out_specs=VMEM,
        scratch_shapes=[
            pltpu.VMEM((ntp - 1, rows, width), jnp.bfloat16),
            pltpu.SemaphoreType.DMA((ntp - 1,)),
            pltpu.SemaphoreType.DMA((ntp - 1,)),
        ],
        compiler_params=pltpu.CompilerParams(collective_id=1 + which, has_side_effects=True),
        name="settle_" + str(which),
    )(
        partial_value.astype(jnp.bfloat16),
        residual_rows,
        norm_gain[which : which + 1],
        norm_bias[which : which + 1],
    )


def heads_kernel(kc, vc, proj_ref, decay_ref, gain_ref, out_ref, prefix, total, state):
    rows = proj_ref.shape[0]
    c = CHUNK
    t_at = lax.broadcasted_iota(jnp.int32, (rows, rows), 0)
    s_at = lax.broadcasted_iota(jnp.int32, (rows, rows), 1)
    lower = ((t_at >= s_at) & (t_at // c == s_at // c)).astype(jnp.float32)
    prefix[...] = jnp.dot(
        lower, decay_ref[...], precision=FULL_ACCURACY, preferred_element_type=jnp.float32
    )
    same = (
        lax.broadcasted_iota(jnp.int32, (kc, vc), 0) // DK
        == lax.broadcasted_iota(jnp.int32, (kc, vc), 1) // DV
    ).astype(jnp.bfloat16)
    turned = (
        lax.broadcasted_iota(jnp.int32, (vc, kc), 0) // DV
        == lax.broadcasted_iota(jnp.int32, (vc, kc), 1) // DK
    ).astype(jnp.float32)
    spot = lax.rem(lax.broadcasted_iota(jnp.int32, (rows, kc), 0), c)
    scale = DK ** (-0.5)
    total[...] = jnp.zeros_like(total)

    def shifted(d, carry):
        q = proj_ref[:, :kc] * scale
        k = pltpu.roll(proj_ref[:, kc : 2 * kc], d, 0)
        v = pltpu.roll(proj_ref[:, 2 * kc : 2 * kc + vc], d, 0)
        g = prefix[...]
        weight = jnp.exp(jnp.where(spot >= d, g - pltpu.roll(g, d, 0), -jnp.inf))
        score = jnp.dot(
            (q * k * weight).astype(jnp.bfloat16), same, preferred_element_type=jnp.float32
        )
        total[...] += score * v
        return carry

    lax.fori_loop(0, c, shifted, 0)
    state[...] = jnp.zeros_like(state)

    def advance(i, carry):
        at = pl.ds(pl.multiple_of(i * c, c), c)
        g = prefix[at, :]
        q = proj_ref[at, :kc] * scale * jnp.exp(g)
        total[at, :] += lax.dot_general(
            q.astype(jnp.bfloat16),
            state[...].astype(jnp.bfloat16),
            (((1,), (1,)), ((), ())),
            preferred_element_type=jnp.float32,
        )
        end = g[c - 1 : c, :]
        k = proj_ref[at, kc : 2 * kc] * jnp.exp(end - g)
        v = proj_ref[at, 2 * kc : 2 * kc + vc]
        fresh = lax.dot_general(
            v.astype(jnp.bfloat16),
            k.astype(jnp.bfloat16),
            (((0,), (0,)), ((), ())),
            preferred_element_type=jnp.float32,
        )
        state[...] = state[...] * jnp.exp(end) + fresh * turned
        return carry

    lax.fori_loop(0, rows // c, advance, 0)
    for head in range(vc // DV):
        cols = slice(head * DV, (head + 1) * DV)
        out = total[:, cols]
        gate = proj_ref[:, 2 * kc + vc + head * DV : 2 * kc + vc + (head + 1) * DV]
        norm = lax.rsqrt(jnp.mean(out * out, -1, keepdims=True) + HEAD_FLOOR)
        value = out * norm * gain_ref[:, cols] * (gate / (1.0 + jnp.exp(-gate)))
        out_ref[:, cols] = value.astype(jnp.bfloat16)


def heads(kc, vc, projected, decay, gain):
    rows = projected.shape[0]
    return pl.pallas_call(
        functools.partial(heads_kernel, kc, vc),
        out_shape=jax.ShapeDtypeStruct((rows, vc), jnp.bfloat16),
        in_specs=[VMEM] * 3,
        out_specs=VMEM,
        scratch_shapes=[
            pltpu.VMEM((rows, kc), jnp.float32),
            pltpu.VMEM((rows, vc), jnp.float32),
            pltpu.VMEM((vc, kc), jnp.float32),
        ],
        name="gla_heads",
    )(projected, decay, gain)


def across(rows, blocks):
    return jnp.concatenate(
        [
            jnp.dot(rows, blocks[at], preferred_element_type=jnp.float32).astype(jnp.bfloat16)
            for at in range(blocks.shape[0])
        ],
        axis=1,
    )


def channel_mix(normed, gate_full, up_full, down_blocks):
    gate_rows = jnp.dot(normed, gate_full, preferred_element_type=jnp.float32)
    up_rows = jnp.dot(normed, up_full, preferred_element_type=jnp.float32)
    hidden = (jax.nn.silu(gate_rows) * up_rows).astype(jnp.bfloat16)
    return across(hidden, down_blocks)


def per_device(
    mesh_shape,
    tokens,
    ffn_gate,
    ffn_up,
    ffn_down,
    query_proj,
    key_proj,
    value_proj,
    outgate_proj,
    output_proj,
    rank_down,
    rank_up,
    decay_bias,
    head_gain,
    norm_gain,
    norm_bias,
):
    ntp = mesh_shape["tp"]
    key_cols = query_proj.shape[1]
    value_cols = value_proj.shape[1]
    joined = jnp.concatenate([query_proj, key_proj, value_proj, outgate_proj], axis=1)
    gathered = gather_all(mesh_shape, [ffn_gate, ffn_up, ffn_down, joined, output_proj])
    gate_full, up_full, joined_full = (
        gathered[at].reshape(-1, gathered[at].shape[2]) for at in (0, 1, 3)
    )
    down_blocks, output_blocks = gathered[2], gathered[4]

    first = settle(
        ntp,
        0,
        channel_mix(tokens, gate_full, up_full, down_blocks),
        tokens,
        0.5,
        norm_gain,
        norm_bias,
    )
    projected = jnp.dot(first, joined_full, preferred_element_type=jnp.float32)
    position = lax.axis_index("tp")
    rank_rows = jnp.dot(first, rank_down, preferred_element_type=jnp.float32)
    up_block = lax.dynamic_slice_in_dim(rank_up, position * key_cols, key_cols, 1)
    bias_block = lax.dynamic_slice_in_dim(decay_bias, position * key_cols, key_cols, 0)
    decay_source = (
        jnp.dot(rank_rows, up_block.astype(jnp.float32), precision=FULL_ACCURACY) + bias_block
    )
    decay_logarithm = jax.nn.log_sigmoid(decay_source) / GATE_SOFTNESS
    gain_block = lax.dynamic_slice_in_dim(head_gain, position * value_cols, value_cols, 0)
    mixed = heads(key_cols, value_cols, projected, decay_logarithm, gain_block[None])
    second = settle(ntp, 1, across(mixed, output_blocks), first, 1.0, norm_gain, norm_bias)
    return settle(
        ntp,
        2,
        channel_mix(second, gate_full, up_full, down_blocks),
        second,
        0.5,
        norm_gain,
        norm_bias,
    )


def solution(mesh):
    return jax.shard_map(
        functools.partial(per_device, dict(mesh.shape)),
        mesh=mesh,
        in_specs=(
            P(("rep", "fs"), None),
            P("fs", "tp"),
            P("fs", "tp"),
            P("tp", "fs"),
            P("fs", "tp"),
            P("fs", "tp"),
            P("fs", "tp"),
            P("fs", "tp"),
            P("tp", "fs"),
            P(),
            P(),
            P(),
            P(),
            P(),
            P(),
        ),
        out_specs=P(("rep", "fs"), None),
        check_vma=False,
    )
```

time: 929 us -> 600 us (0.65); the launches traced: 917 us -> 600 us
  waiting for transfers between devices: 709 us -> 0 us
  Pallas kernels: 0 us -> 530 us
  matrix products: 135 us -> 60 us
  other arithmetic: 39.5 us -> 2.06 us
  starting transfers between devices: 14.8 us -> 0 us
  between operations: 13.9 us -> 0.41 us
    all_gather x8 -> x0, waiting for transfers between devices: 660 us -> none  [the longest x1 164 us: per_device(): down_full = lax.all_gather(ffn_down, 'fs', axis=1, tiled=True)]
    pallas_call x0 -> x5, Pallas kernels: none -> 530 us  [the longest x1 484 us: gather_all(): pl.pallas_call(functools.partial(gather_kernel, nz, ny, count), out_shape...]
    dot_general x20 -> x27, matrix products: 112 us -> 39.3 us  [the longest x24 25.1 us: across(): jnp.dot(rows, blocks[at], preferred_element_type=jnp.float32)]
    psum x3 -> x0, waiting for transfers between devices: 43.8 us -> none  [settle(): lax.psum(partial_value.astype(jnp.bfloat16), 'tp').astype(jnp.float32)]
    dot_general x4 -> x0, other arithmetic: 23.6 us -> none  [advance(): jnp.einsum('lshk,lhk,shk->hls', weight, query_block, key_block, precision...]
    psum x3 -> x0, starting transfers between devices: 14.5 us -> none  [settle(): lax.psum(partial_value.astype(jnp.bfloat16), 'tp').astype(jnp.float32)]
  transfers between devices with their start and end apart: 11 -> 0, of which waited for: 10 -> 0; matrix products, arithmetic and copies ran while one was open for 14% -> 0% of each run, Pallas kernels for 0% -> 0%
where the time goes in v1:
time: 600 us
  Pallas kernels  530 us (88%)
  matrix products  60 us (10%)
  local copies, waits for them, and re-layouts  7.45 us (1%)
    pallas_call x1, Pallas kernels, gather_all(): pl.pallas_call(functools.partial(gather_kernel, nz, ny, count), out_shape...  484 us
    pallas_call x3, Pallas kernels, settle(): pl.pallas_call(functools.partial(settle_kernel, ntp, factor), out_shape=j...  29.3 us
    dot_general x24, matrix products, across(): jnp.dot(rows, blocks[at], preferred_element_type=jnp.float32)  25.1 us
    pallas_call x1, Pallas kernels, heads(): pl.pallas_call(functools.partial(heads_kernel, kc, vc), out_shape=jax.Sha...  16.5 us
    dot_general x2, matrix products, channel_mix(): gate_rows = jnp.dot(normed, gate_full, preferred_element_type=jnp.float32)  14.2 us
    dot_general x2, matrix products, channel_mix(): up_rows = jnp.dot(normed, up_full, preferred_element_type=jnp.float32)  13.1 us

profile of v1, /device:TPU:25, one launch (start us, length us, event | category | flops | bytes accessed | tf_op | source)
XLA Modules:
  0.0 599.7 jit_solution(12108591016216866357)
XLA Ops:
  0.0 2.1 pad_maximum_fusion.refs_3_
  2.1 483.9 %gather_weights.1 = (bf16[8,256,2816]{2,1,0:T(8,128)(2,1)}, bf16[8,256,2816]{2,1,0:T(8,128)(2,1)}, bf16[8,2816,256]{2,1,0:T(8,128)(2,1)}, bf16[8,256,1536]{2,1,0:T(8,128)(2,1)}, bf16[8,512,256]{2,1,0:T(8,128)(2,1)}) custom-call(bf16[256,2816]{1,0:T(8,128)(2,1)} %refs_0_.1, bf16[256,2816]{1,0:T(8,128)(2,1)} %refs_1_.1, bf16[2816,256]{1,0:T(8,128)(2,1)} %refs_2_.1, ...), custom_call_target="tpu_custom_call" | custom-call | tf_op jit(solution)/shard_map/gather_weights/pallas_call | solution.py:150
  486.1 6.3 %convolution_bitcast_fusion.1 = f32[256,2816]{0,1:T(8,128)S(1)} fusion(bf16[2048,2816]{1,0:T(8,128)(2,1)} %bitcast.182, bf16[256,2048]{1,0:T(8,128)(2,1)S(1)} %copy-done.4), kind=kOutput, calls=%fused_computation.2 | convolution fusion | flops 2952790016 | bytes 15466496 | tf_op jit(solution)/shard_map/dot_general | solution.py:317
  492.4 1.3 copy-done.13
  493.6 4.0 fusion.2
  503.6 11.7 %settle_0.1.rest_ref = bf16[256,2048]{1,0:T(8,128)(2,1)} custom-call(bf16[256,2048]{1,0:T(8,128)(2,1)} %copy-done.5, bf16[256,2048]{1,0:T(8,128)(2,1)} %rest_ref.1, f32[1,2048]{1,0:T(1,128)} %get-tuple-element.22.gain_ref, f32[1,2048]{1,0:T(1,128)} %get-tuple-element.16.shift_ref), custom_call_target="tpu_custom_call" | custom-call | tf_op jit(solution)/shard_map/settle_0/pallas_call | solution.py:202
  515.3 6.1 %fusion.178.proj_ref = f32[256,1536]{1,0:T(8,128)} fusion(bf16[256,2048]{1,0:T(8,128)(2,1)} %settle_0.1.rest_ref, bf16[2048,1536]{1,0:T(8,128)(2,1)} %bitcast.184), kind=kOutput, calls=%fused_computation.128 | convolution fusion | flops 1610612736 | bytes 8912896 | tf_op jit(solution)/shard_map/dot_general | solution.py:360
  523.7 16.5 %gla_heads.1 = bf16[256,512]{1,0:T(8,128)(2,1)} custom-call(f32[256,1536]{1,0:T(8,128)} %fusion.178.proj_ref, f32[256,256]{1,0:T(8,128)} %fusion.157.decay_ref, f32[1,512]{1,0:T(1,128)} %bitcast.177), custom_call_target="tpu_custom_call" | custom-call | tf_op jit(solution)/shard_map/gla_heads/pallas_call | solution.py:292
  540.2 1.2 fusion.155
  541.5 1.2 fusion.154
  542.6 1.2 fusion.153
  546.0 8.7 %settle_1.1.rest_ref = bf16[256,2048]{1,0:T(8,128)(2,1)} custom-call(bf16[256,2048]{1,0:T(8,128)(2,1)} %copy-done.6, bf16[256,2048]{1,0:T(8,128)(2,1)} %settle_0.1.rest_ref, f32[1,2048]{1,0:T(1,128)} %get-tuple-element.21.gain_ref, f32[1,2048]{1,0:T(1,128)} %get-tuple-element.17.shift_ref), custom_call_target="tpu_custom_call" | custom-call | tf_op jit(solution)/shard_map/settle_1/pallas_call | solution.py:202
  554.7 7.9 %fusion.180 = f32[256,2816]{0,1:T(8,128)S(1)} fusion(bf16[256,2048]{1,0:T(8,128)(2,1)} %settle_1.1.rest_ref, bf16[2048,2816]{1,0:T(8,128)(2,1)} %bitcast.183), kind=kOutput, calls=%fused_computation.130 | convolution fusion | flops 2952790016 | bytes 15466496 | tf_op jit(solution)/shard_map/dot_general | solution.py:317
  562.6 9.2 %fusion = bf16[256,2816]{0,1:T(8,128)(2,1)S(1)} fusion(bf16[256,2048]{1,0:T(8,128)(2,1)S(1)} %copy-done.3, bf16[2048,2816]{1,0:T(8,128)(2,1)} %bitcast.180, f32[256,2816]{0,1:T(8,128)S(1)} %fusion.180), kind=kOutput, calls=%fused_computation.3 | convolution fusion | flops 2957115392 | bytes 16908288 | tf_op jit(solution)/shard_map/dot_general | solution.py:318
  571.8 2.0 fusion.61
  573.8 2.0 fusion.73
  575.7 2.0 fusion.85
  577.7 2.0 fusion.97
  579.7 2.0 fusion.109
  581.6 2.0 fusion.121
  583.6 2.0 fusion.133
  585.5 2.0 fusion.145.part_ref
  588.5 8.9 %settle_2.1 = bf16[256,2048]{1,0:T(8,128)(2,1)} custom-call(bf16[256,2048]{1,0:T(8,128)(2,1)} %copy-done.7, bf16[256,2048]{1,0:T(8,128)(2,1)} %settle_1.1.rest_ref, f32[1,2048]{1,0:T(1,128)} %get-tuple-element.23.gain_ref, f32[1,2048]{1,0:T(1,128)} %get-tuple-element.15.shift_ref), custom_call_target="tpu_custom_call" | custom-call | tf_op jit(solution)/shard_map/settle_2/pallas_call | solution.py:202
  597.4 2.3 copy.91
  (56 shorter events, 11.2 us)
Async XLA Ops:
  0.0 521.5 %copy-start = (bf16[2048,16]{0,1:T(8,128)(2,1)S(1)}, bf16[2048,16]{0,1:T(8,128)(2,1)}, u32[]{:S(2)}) copy-start(bf16[2048,16]{0,1:T(8,128)(2,1)} %param.24) | copy-start | bytes 196612
  2.1 484.0 %copy-start.4 = (bf16[256,2048]{1,0:T(8,128)(2,1)S(1)}, bf16[256,2048]{1,0:T(8,128)(2,1)}, u32[]{:S(2)}) copy-start(bf16[256,2048]{1,0:T(8,128)(2,1)} %rest_ref.1) | copy-start | bytes 3145732
  486.0 7.6 %copy-start.13 = (bf16[8,256,2816]{2,1,0:T(8,128)(2,1)S(1)}, bf16[8,256,2816]{2,1,0:T(8,128)(2,1)}, u32[]{:S(2)}) copy-start(bf16[8,256,2816]{2,1,0:T(8,128)(2,1)} %get-tuple-element.11) | copy-start | bytes 34603012
  486.0 11.6 %slice-start = ((s8[11534336]{0:T(1024)(128)(4,1)}), s8[4194304]{0:T(1024)(128)(4,1)S(1)}, s32[]{:S(2)}) async-start(s8[11534336]{0:T(1024)(128)(4,1)} %bitcast.178), calls=%async_computation | async-start | bytes 8388608
  486.0 11.6 %slice-start.1 = ((s8[11534336]{0:T(1024)(128)(4,1)}), s8[4194304]{0:T(1024)(128)(4,1)S(1)}, s32[]{:S(2)}) async-start(s8[11534336]{0:T(1024)(128)(4,1)} %bitcast.178), calls=%async_computation.1 | async-start | bytes 8388608
  493.6 4.0 slice-start.2
  501.8 0.8 copy-start.9
  501.8 0.8 copy-start.10
  502.6 1.0 copy-start.5
  515.3 6.2 %copy-start.2 = (bf16[256,2048]{1,0:T(8,128)(2,1)S(1)}, bf16[256,2048]{1,0:T(8,128)(2,1)}, u32[]{:S(2)}) copy-start(bf16[256,2048]{1,0:T(8,128)(2,1)} %settle_0.1.rest_ref) | copy-start | bytes 3145732
  515.3 6.6 %copy-start.12 = (f32[512]{0:T(512)S(1)}, f32[512]{0:T(512)}, u32[]{:S(2)}) copy-start(f32[512]{0:T(512)} %param.26) | copy-start | bytes 6148
  515.3 6.7 %copy-start.15 = (bf16[16,512]{1,0:T(8,128)(2,1)S(1)}, bf16[16,512]{1,0:T(8,128)(2,1)}, u32[]{:S(2)}) copy-start(bf16[16,512]{1,0:T(8,128)(2,1)} %param.25) | copy-start | bytes 49156
  521.5 1.6 copy-start.11
  521.9 18.3 %copy-start.14 = (bf16[8,512,256]{2,1,0:T(8,128)(2,1)S(1)}, bf16[8,512,256]{2,1,0:T(8,128)(2,1)}, u32[]{:S(2)}) copy-start(bf16[8,512,256]{2,1,0:T(8,128)(2,1)} %get-tuple-element.14) | copy-start | bytes 6291460
  540.2 3.6 copy-start.8
  545.0 1.0 copy-start.6
  554.7 7.9 %copy-start.3 = (bf16[256,2048]{1,0:T(8,128)(2,1)S(1)}, bf16[256,2048]{1,0:T(8,128)(2,1)}, u32[]{:S(2)}) copy-start(bf16[256,2048]{1,0:T(8,128)(2,1)} %settle_1.1.rest_ref) | copy-start | bytes 3145732
  587.5 1.0 copy-start.7
  588.5 11.2 %copy-start.1 = (bf16[2048,16]{0,1:T(8,128)(2,1)S(1)}, bf16[2048,16]{0,1:T(8,128)(2,1)}, u32[]{:S(2)}) copy-start(bf16[2048,16]{0,1:T(8,128)(2,1)} %param.24) | copy-start | bytes 196612
